TPU v7x, 32 devices: a whole 2x2x4 slice. The times are simulated.
32 devices in a mesh: sp: 8 (over z, y), tp: 4 (over x, core).
Axes of the slice: x: 2, y: 2, z: 4, core: 2. Of those that a mesh axis runs over, the one named last changes fastest.
Arguments:
- query_nope: bfloat16 [1536, 4096], P('sp', 'tp'), may hold values from -6 to 6
- query_rope: bfloat16 [1536, 2048], P('sp', 'tp'), may hold values from -24 to 24
- latent: bfloat16 [1536, 512], P('sp'), may hold values from -6 to 6
- key_rope: bfloat16 [1536, 32], P('sp'), may hold values from -24 to 24
- latent_gain: float32 [512], replicated, may hold values from 0.1 to 1.9
- key_up: bfloat16 [512, 4096], P(None, 'tp'), may hold values from -0.25 to 0.25
- value_up: bfloat16 [512, 4096], P(None, 'tp'), may hold values from -0.25 to 0.25
- out_proj: bfloat16 [4096, 4096], P('tp'), may hold values from -0.09375 to 0.09375
- resid: bfloat16 [1536, 4096], P(('sp', 'tp')), may hold values from -6 to 6
- attn_gain: float32 [4096], replicated, may hold values from 0.1 to 1.9
- pre_gain: float32 [4096], replicated, may hold values from 0.1 to 1.9
- routes: int32 [1536, 2], P(('sp', 'tp')), may hold values from 0 to 7, all different within a row; in each aligned block of 48 rows (0 to 47, 48 to 95, ...) at most 24 rows name the same one
- route_weights: float32 [1536, 2], P(('sp', 'tp')), may hold values from 0.2 to 2
- expert_gate: bfloat16 [8, 4096, 1024], P('sp', None, 'tp'), may hold values from -0.09375 to 0.09375
- expert_up: bfloat16 [8, 4096, 1024], P('sp', None, 'tp'), may hold values from -0.09375 to 0.09375
- expert_down: bfloat16 [8, 1024, 4096], P('sp', 'tp'), may hold values from -0.1875 to 0.1875
- shared_gate: bfloat16 [4096, 1024], P(None, 'tp'), may hold values from -0.09375 to 0.09375
- shared_up: bfloat16 [4096, 1024], P(None, 'tp'), may hold values from -0.09375 to 0.09375
- shared_down: bfloat16 [1024, 4096], P('tp'), may hold values from -0.1875 to 0.1875
- moe_gain: float32 [4096], replicated, may hold values from 0.1 to 1.9
Outputs:
- output: bfloat16 [1536, 4096], P(('sp', 'tp'))
Inputs may be any that keep to these rules, and one draw needn't show every extreme that they name: `routes`: A row names 2 different experts. In each aligned block of 48 rows no expert is named by more than 24 rows, and in some block an expert is named by exactly 24 rows.
All inputs are finite; a program needn't handle non-finite values.
Results may differ from a plain program's by a relative error of at most 0.018.
Values may be sent and summed in bfloat16 or wider, within the bound.
A program may use at most 128 MiB of HBM per device.

v0:
```python
import math
import jax
import jax.numpy as jnp
from jax import lax
from jax.sharding import PartitionSpec as P

MODEL_DIM = 4096
NOPE_DIM = 64
ROPE_DIM = 32
VALUE_DIM = 64
TOP_K = 2
epsilon = 1e-06
theta_base = 10000.0


def rms_scale(values, gain_vector):
    return (
        values
        * lax.rsqrt(jnp.mean(values * values, axis=-1, keepdims=True) + epsilon)
        * gain_vector
    )


def rotate(values, positions):
    half_dim = values.shape[-1] // 2
    inverse = theta_base ** (-jnp.arange(half_dim, dtype=jnp.float32) / half_dim)
    angles = positions.astype(jnp.float32)[..., None] * inverse
    cosine = jnp.cos(angles)
    sine_part = jnp.sin(angles)
    first_half = values[..., :half_dim]
    second_half = values[..., half_dim:]
    return jnp.concatenate(
        [
            first_half * cosine - second_half * sine_part,
            second_half * cosine + first_half * sine_part,
        ],
        axis=-1,
    )


def expert_block(expert_in, gate_part, up_part, down_part):
    hidden = (
        jax.nn.silu(jnp.dot(expert_in, gate_part, preferred_element_type=jnp.float32))
        * jnp.dot(expert_in, up_part, preferred_element_type=jnp.float32)
    ).astype(jnp.bfloat16)
    return jnp.dot(hidden, down_part, preferred_element_type=jnp.float32).astype(jnp.bfloat16)


def dispatch_table(normed_rows, route_rows, experts, capacity):
    row_count = normed_rows.shape[0]
    flat_routes = route_rows.reshape(-1)
    onehot = (flat_routes[:, None] == jnp.arange(experts, dtype=jnp.int32)[None, :]).astype(
        jnp.int32
    )
    earlier = jnp.cumsum(onehot, axis=0) - onehot
    target = flat_routes * capacity + jnp.sum(earlier * onehot, axis=1)
    matches = (
        target.reshape(row_count, -1)[None, :, :]
        == jnp.arange(experts * capacity, dtype=jnp.int32)[:, None, None]
    )
    spread = jnp.any(matches, axis=2).astype(jnp.bfloat16)
    slot_table = jnp.dot(spread, normed_rows, preferred_element_type=jnp.float32).astype(
        jnp.bfloat16
    )
    return (slot_table.reshape(experts, capacity, normed_rows.shape[1]), target)


def on_device(
    query_nope,
    query_rope,
    latent,
    key_rope,
    latent_gain,
    key_up,
    value_up,
    out_proj,
    resid,
    attn_gain,
    pre_gain,
    routes,
    route_weights,
    expert_gate,
    expert_up,
    expert_down,
    shared_gate,
    shared_up,
    shared_down,
    moe_gain,
):
    local_rows = query_nope.shape[0]
    heads_here = query_nope.shape[1] // NOPE_DIM
    query_pos = lax.axis_index("sp") * local_rows + jnp.arange(local_rows, dtype=jnp.int32)
    last_query = lax.axis_index("sp") * local_rows + local_rows - 1
    query_rot = rotate(
        query_rope.astype(jnp.float32).reshape(local_rows, heads_here, ROPE_DIM), query_pos[:, None]
    ).astype(jnp.bfloat16)
    key_rot = rotate(key_rope.astype(jnp.float32), query_pos).astype(jnp.bfloat16)
    latent_normed = rms_scale(latent.astype(jnp.float32), latent_gain).astype(jnp.bfloat16)
    query_heads = query_nope.reshape(local_rows, heads_here, NOPE_DIM)
    score_scale = (NOPE_DIM + ROPE_DIM) ** (-0.5)

    def attend(state_now, latent_rows, rotary_rows, key_start):
        piece_rows = latent_rows.shape[0]
        keys_here = jnp.dot(latent_rows, key_up, preferred_element_type=jnp.float32).astype(
            jnp.bfloat16
        )
        keys_here = keys_here.reshape(piece_rows, heads_here, NOPE_DIM)
        values_here = jnp.dot(latent_rows, value_up, preferred_element_type=jnp.float32).astype(
            jnp.bfloat16
        )
        values_here = values_here.reshape(piece_rows, heads_here, VALUE_DIM)
        scores = (
            jnp.einsum("qhd,khd->hqk", query_heads, keys_here, preferred_element_type=jnp.float32)
            + jnp.einsum("qhr,kr->hqk", query_rot, rotary_rows, preferred_element_type=jnp.float32)
        ) * score_scale
        allowed = (key_start + jnp.arange(piece_rows, dtype=jnp.int32))[None, :] <= query_pos[
            :, None
        ]
        scores = jnp.where(allowed[None], scores, -1e30)
        running, total_sum, summed = state_now
        newest = jnp.maximum(running, jnp.max(scores, axis=-1))
        factor = jnp.exp(running - newest)
        exponent = jnp.exp(scores - newest[..., None])
        total_sum = total_sum * factor + jnp.sum(exponent, axis=-1)
        summed = summed * factor[..., None] + jnp.einsum(
            "hqk,khd->hqd",
            exponent.astype(jnp.bfloat16),
            values_here,
            preferred_element_type=jnp.float32,
        )
        return (newest, total_sum, summed)

    initial = (
        jnp.full((heads_here, local_rows), -1e30, jnp.float32),
        jnp.zeros((heads_here, local_rows), jnp.float32),
        jnp.zeros((heads_here, local_rows, VALUE_DIM), jnp.float32),
    )
    latent_piece = lax.all_gather(latent_normed, "sp", axis=0, tiled=True)
    rotary_piece = lax.all_gather(key_rot, "sp", axis=0, tiled=True)
    piece_rows = latent_piece.shape[0]
    step_rows = math.gcd(piece_rows, 512)

    def one_step(step_index, inner_state):
        offset = step_index * step_rows
        latent_rows = lax.dynamic_slice_in_dim(latent_piece, offset, step_rows, 0)
        rotary_rows = lax.dynamic_slice_in_dim(rotary_piece, offset, step_rows, 0)
        return lax.cond(
            offset <= last_query,
            lambda carried: attend(carried, latent_rows, rotary_rows, offset),
            lambda carried: carried,
            inner_state,
        )

    running, total_sum, summed = lax.fori_loop(0, piece_rows // step_rows, one_step, initial)
    attention = (
        (summed / total_sum[..., None])
        .transpose(1, 0, 2)
        .reshape(local_rows, heads_here * VALUE_DIM)
    )
    attention = attention.astype(jnp.bfloat16)
    projected = lax.psum_scatter(
        jnp.dot(attention, out_proj, preferred_element_type=jnp.float32).astype(jnp.bfloat16),
        "tp",
        scatter_dimension=0,
        tiled=True,
    ).astype(jnp.float32)
    mixed = (resid.astype(jnp.float32) + rms_scale(projected, attn_gain)).astype(jnp.bfloat16)
    normed = rms_scale(mixed.astype(jnp.float32), pre_gain).astype(jnp.bfloat16)
    rows_here = resid.shape[0]
    tp_count = lax.axis_size("tp")
    experts = lax.axis_size("sp")
    capacity = max(2, 2 * rows_here * TOP_K // experts)
    own_table, target = dispatch_table(normed, routes, experts, capacity)
    arrived = lax.all_to_all(own_table, "sp", split_axis=0, concat_axis=0, tiled=True)
    column = lax.all_gather(arrived[None], "tp", axis=0, tiled=True)
    group_normed = lax.all_gather(normed, "tp", axis=0, tiled=True)
    expert_out = expert_block(
        column.reshape(-1, MODEL_DIM), expert_gate[0], expert_up[0], expert_down[0]
    )
    shared_part = expert_block(group_normed, shared_gate, shared_up, shared_down)
    routed_sum, shared_sum = (
        lax.psum_scatter(
            expert_out.reshape(column.shape).astype(jnp.float32).astype(jnp.bfloat16),
            "tp",
            scatter_dimension=0,
            tiled=True,
        ).astype(jnp.float32),
        lax.psum_scatter(
            shared_part.reshape(tp_count, rows_here, MODEL_DIM)
            .astype(jnp.float32)
            .astype(jnp.bfloat16),
            "tp",
            scatter_dimension=0,
            tiled=True,
        ).astype(jnp.float32),
    )
    expert_rows = lax.all_to_all(
        routed_sum.astype(jnp.bfloat16), "sp", split_axis=1, concat_axis=1, tiled=True
    ).reshape(-1, MODEL_DIM)
    shared_out = shared_sum.reshape(rows_here, MODEL_DIM)
    picked = expert_rows[target].astype(jnp.float32).reshape(rows_here, TOP_K, MODEL_DIM)
    routed = jnp.sum(picked * route_weights[..., None], axis=1)
    moe = shared_out + routed
    return (mixed.astype(jnp.float32) + rms_scale(moe, moe_gain)).astype(jnp.bfloat16)


def solution(mesh):
    in_specs = (
        P("sp", "tp"),
        P("sp", "tp"),
        P("sp", None),
        P("sp", None),
        P(),
        P(None, "tp"),
        P(None, "tp"),
        P("tp", None),
        P(("sp", "tp"), None),
        P(),
        P(),
        P(("sp", "tp"), None),
        P(("sp", "tp"), None),
        P("sp", None, "tp"),
        P("sp", None, "tp"),
        P("sp", "tp", None),
        P(None, "tp"),
        P(None, "tp"),
        P("tp", None),
        P(),
    )
    out_specs = P(("sp", "tp"), None)
    return jax.shard_map(
        on_device, mesh=mesh, in_specs=in_specs, out_specs=out_specs, check_vma=False
    )
```

profile of v0, /device:TPU:0, one launch (start us, length us, event | category | flops | bytes accessed | tf_op | source)
XLA Modules:
  0.0 459.1 jit_solution(2781892771527778260)
XLA Ops:
  6.5 1.2 fusion.46
  7.8 1.7 fusion.48
  9.5 0.0 reduce-scatter.4.cloned.1.call-start
  9.6 0.7 convert_element_type.118
  10.3 1.1 copy.67
  11.4 0.1 multiply_cosine_fusion
  11.5 32.8 %all-gather.1 = bf16[8,192,32]{1,2,0:T(8,128)(2,1)S(1)} all-gather(bf16[1,192,32]{1,2,0:T(8,128)(2,1)S(1)} %maximum_bitcast_fusion), channel_id=1, replica_groups=mesh['sp'=8,'tp'=4] {'sp'}, dimensions={0}, use_global_device_ids=true | all-gather | bytes 110592 | tf_op jit(solution)/shard_map/all_gather | solution.py:139
  44.3 0.1 copy.66
  44.4 0.8 reshape.263
  45.2 1.0 copy.65
  46.2 0.1 subtract_convert_fusion
  46.3 10.5 %all-gather.6.cloned.1.call-done = bf16[1536,512]{1,0:T(8,128)(2,1)} async-done(((bf16[192,512]{1,0:T(8,128)(2,1)}), bf16[1536,512]{1,0:T(8,128)(2,1)}) %all-gather.6.cloned.1.call-update) | async-done | bytes 1572880 | tf_op jit(solution)/shard_map/all_gather | solution.py:138
  56.8 1.2 broadcast_in_dim.34
  58.0 22.1 %while.18 = (s32[]{:T(128)}, f32[16,192]{1,0:T(8,128)S(1)}, f32[16,192]{1,0:T(8,128)S(1)}, f32[16,192,64]{1,2,0:T(8,128)}, s32[]{:T(128)}, /*index=5*/bf16[1536,...) while((s32[]{:T(128)}, f32[16,192]{1,0:T(8,128)S(1)}, ...), condition=%wide.region_6.7_spmd.clone, body=%wide.region_1.6_spmd.clone.sunk | while | flops 1591188224 | bytes 74948008 | solution.py:154
  58.0 22.1 %conditional.3 = ((f32[16,192]{1,0:T(8,128)S(1)}, f32[16,192]{1,0:T(8,128)S(1)}, f32[16,192,64]{1,2,0:T(8,128)})) conditional(s32[]{:T(128)} %convert_element_type.198, (f32[16,192]{1,0:T(8,128)S(1)}, f32[16,192]{1,0:T(8,128)S(1)}, f32[16,192,64]{1,2,0:T(8,128)}) %tuple.60, (s32[]{:T(128)}, s32[]{:T(128)}, bf16[1536,512]{1,0:T(8,128)(2,1)}, ...), branch_computations={%region_2.0_spmd, %region_3.5_spmd} | conditional | flops 1591188224 | bytes 74946960 | solution.py:147
  58.0 3.1 convolution_convert_fusion.1
  61.1 1.5 copy.63
  62.6 2.1 fusion.64
  64.7 0.1 broadcast_compare_fusion
  64.8 2.9 fusion.63
  67.7 1.6 fusion.5
  69.3 1.0 copy-done.1
  70.3 2.8 convolution_convert_fusion
  73.1 1.5 copy.64
  74.6 5.4 %fusion.9 = f32[16,192,64]{1,2,0:T(8,128)} fusion(bf16[512,16,64]{0,2,1:T(8,128)(2,1)S(1)} %bitcast.74, f32[16,192,512]{2,1,0:T(8,128)} %copy-done.1, f32[16,192]{1,0:T(8,128)S(1)} %max.5, f32[16,192,64]{1,2,0:T(8,128)} %get-tuple-element.325, f32[16,192]{1,0:T(8,128)S(1)} %get-tuple-element.405), kind=kOutput, calls=%fused_computation.12 | convolution fusion | flops 204865536 | bytes 8937472 | tf_op jit(solution)/shard_map/while/body/eval_jaxpr/cond/branch_1_fun/hqk,khd->hqd/dot_general | solution.py:125
  80.1 1.3 divide_convert_fusion
  81.4 6.4 %convolution_convert_fusion.5 = bf16[192,4096]{1,0:T(8,128)(2,1)} fusion(bf16[192,1024]{0,1:T(8,128)(2,1)S(1)} %bitcast.80, bf16[1024,4096]{1,0:T(8,128)(2,1)} %param.31), kind=kOutput, calls=%fused_computation.28 | convolution fusion | flops 1611399168 | bytes 10354688 | tf_op jit(solution)/shard_map/dot_general | solution.py:162
  87.9 0.0 all-gather.10.cloned.1.call-start
  87.9 0.1 copy.68
  88.0 0.1 eq.28
  88.1 0.1 fusion.57
  88.2 0.1 reduce_window_sum.11
  88.4 0.2 select_reduce_fusion
  88.5 0.1 reduce_sum.74
  88.7 0.1 copy.70
  88.8 0.1 fusion.56
  88.9 69.8 %reduce-scatter.4.cloned.1.call-done = bf16[48,4096]{1,0:T(8,128)(2,1)} async-done(((bf16[192,4096]{1,0:T(8,128)(2,1)}), bf16[48,4096]{1,0:T(8,128)(2,1)}) %reduce-scatter.4.cloned.1.call-update) | async-done | bytes 393232 | tf_op jit(solution)/shard_map/reduce_scatter | solution.py:161
  158.6 1.2 fusion.33
  159.8 1.4 fusion.37
  161.2 0.2 fusion.39
  161.4 0.6 convolution_convert_fusion.3
  162.0 42.3 %all_to_all.10 = bf16[8,24,4096]{2,1,0:T(8,128)(2,1)} all-to-all(bf16[8,24,4096]{2,1,0:T(8,128)(2,1)S(1)} %bitcast.79), channel_id=1, replica_groups=mesh['sp'=8,'tp'=4] {'sp'}, dimensions={0} | all-to-all | bytes 3145728 | tf_op jit(solution)/shard_map/all_to_all | solution.py:174
  204.3 0.5 all-gather.8.cloned.1.call-update
  204.9 0.2 all-reduce.3.cloned.1.call-start
  205.1 43.8 %all-gather.10.cloned.1.call-done = bf16[32,24,4096]{2,1,0:T(8,128)(2,1)} async-done(((bf16[8,24,4096]{2,1,0:T(8,128)(2,1)}), bf16[32,24,4096]{2,1,0:T(8,128)(2,1)}) %all-gather.10.cloned.1.call-update) | async-done | bytes 6291472 | tf_op jit(solution)/shard_map/all_gather | solution.py:175
  248.9 6.1 %fusion.22 = f32[768,256]{1,0:T(8,128)} fusion(bf16[768,4096]{1,0:T(8,128)(2,1)} %bitcast.82, bf16[1,4096,256]{2,1,0:T(8,128)(2,1)} %param.37), kind=kOutput, calls=%fused_computation.32 | convolution fusion | flops 1610612736 | bytes 9175040 | tf_op jit(solution)/shard_map/dot_general | solution.py:43
  255.0 13.3 %convolution_convert_fusion.2 = bf16[768,4096]{1,0:T(8,128)(2,1)} fusion(bf16[1,256,4096]{2,1,0:T(8,128)(2,1)S(1)} %copy-done, bf16[768,4096]{1,0:T(8,128)(2,1)} %bitcast.83, bf16[1,4096,256]{2,1,0:T(8,128)(2,1)} %param.38, f32[768,256]{1,0:T(8,128)} %fusion.22), kind=kOutput, calls=%fused_computation.25 | convolution fusion | flops 3225550848 | bytes 17563648 | tf_op jit(solution)/shard_map/dot_general | solution.py:46
  268.2 6.3 %copy.71 = bf16[4,8,24,4096]{3,2,0,1:T(8,128)(2,1)} copy(bf16[4,8,24,4096]{3,2,1,0:T(8,128)(2,1)} %bitcast.77) | data formatting | bytes 12582912 | tf_op jit(solution)/shard_map/reshape | solution.py:183
  274.5 0.0 reduce-scatter.6.cloned.1.call-start
  274.6 0.6 copy-done.11
  275.1 0.6 dynamic-slice
  275.8 2.6 fusion.65
  278.4 6.9 %convolution_convert_fusion.4 = bf16[192,4096]{1,0:T(8,128)(2,1)} fusion(bf16[256,4096]{1,0:T(8,128)(2,1)} %param.42, bf16[192,4096]{1,0:T(8,128)(2,1)} %all-gather.8.cloned.1.call-done, bf16[4096,256]{1,0:T(8,128)(2,1)} %param.41, f32[192,256]{1,0:T(8,128)S(1)} %fusion.65), kind=kOutput, calls=%fused_computation.27 | convolution fusion | flops 806387712 | bytes 7536640 | tf_op jit(solution)/shard_map/dot_general | solution.py:46
  285.3 108.8 %all-reduce.3.cloned.1.call-done = bf16[4,8,24,4096]{3,2,0,1:T(8,128)(2,1)} async-done(((bf16[4,8,24,4096]{3,2,0,1:T(8,128)(2,1)}), bf16[4,8,24,4096]{3,2,0,1:T(8,128)(2,1)}) %all-reduce.3.cloned.1.call-update) | async-done | bytes 6291472
  394.2 3.3 constant_dynamic-slice_fusion
  397.5 5.6 %all-to-all-start.1 = ((bf16[1,8,24,4096]{3,2,0,1:T(8,128)(2,1)}), bf16[1,8,24,4096]{3,2,0,1:T(8,128)(2,1)}, u32[]{:S(2)}, u32[]{:S(2)}) async-start(bf16[1,8,24,4096]{3,2,0,1:T(8,128)(2,1)} %constant_dynamic-slice_fusion), calls=%async_computation.3 | async-start | bytes 3145728 | tf_op jit(solution)/shard_map/all_to_all | solution.py:197
  403.1 0.1 mul.260
  403.3 0.1 copy.72
  403.4 36.5 %all-to-all-done.1 = bf16[1,8,24,4096]{3,2,0,1:T(8,128)(2,1)} async-done(((bf16[1,8,24,4096]{3,2,0,1:T(8,128)(2,1)}), bf16[1,8,24,4096]{3,2,0,1:T(8,128)(2,1)}, u32[]{:S(2)}, u32[]{:S(2)}) %all-to-all-start.1) | async-done | bytes 1572896 | tf_op jit(solution)/shard_map/all_to_all | solution.py:197
  439.8 3.4 gather_fusion
  443.2 2.1 reshape.251
  445.4 3.6 multiply_reduce_fusion
  449.1 1.2 multiply_reduce_fusion.1
  450.3 1.9 fusion.40
  (54 shorter events, 0.4 us)
Async XLA Ops:
  6.5 248.4 %copy-start = (bf16[1,256,4096]{2,1,0:T(8,128)(2,1)S(1)}, bf16[1,256,4096]{2,1,0:T(8,128)(2,1)}, u32[]{:S(2)}) copy-start(bf16[1,256,4096]{2,1,0:T(8,128)(2,1)} %param.39) | copy-start | bytes 6291460
  6.5 38.6 %copy-start.3 = (bf16[192,1024]{1,0:T(8,128)(2,1)S(1)}, bf16[192,1024]{1,0:T(8,128)(2,1)}, u32[]{:S(2)}) copy-start(bf16[192,1024]{1,0:T(8,128)(2,1)} %param.24) | copy-start | bytes 1179652
  6.5 50.3 %all-gather.6.cloned.1.call-start = ((), (), s32[]{:S(2)}) async-start(), calls=%async_computation.4 | async-start | bytes 1769472 | tf_op jit(solution)/shard_map/all_gather | solution.py:138
  9.5 149.1 %reduce-scatter.4.cloned.1.call-start = ((), (), s32[]{:S(2)}) async-start(), calls=%async_computation.5 | async-start | bytes 1966080 | tf_op jit(solution)/shard_map/reduce_scatter | solution.py:161
  67.7 2.6 copy-start.1
  67.7 2.6 copy-start.10
  81.4 6.5 %copy-start.8 = (s32[48,2]{0,1:T(2,128)S(1)}, s32[48,2]{0,1:T(2,128)}, u32[]{:S(2)}) copy-start(s32[48,2]{0,1:T(2,128)} %param.35) | copy-start | bytes 1156
  87.8 72.0 %copy-start.4 = (bf16[48,4096]{1,0:T(8,128)(2,1)S(1)}, bf16[48,4096]{1,0:T(8,128)(2,1)}, u32[]{:S(2)}) copy-start(bf16[48,4096]{1,0:T(8,128)(2,1)} %param.32) | copy-start | bytes 1179652
  87.8 72.0 %copy-start.5 = (f32[4096]{0:T(1024)S(1)}, f32[4096]{0:T(1024)}, u32[]{:S(2)}) copy-start(f32[4096]{0:T(1024)} %param.33) | copy-start | bytes 49156
  87.8 73.4 %copy-start.7 = (f32[4096]{0:T(1024)S(1)}, f32[4096]{0:T(1024)}, u32[]{:S(2)}) copy-start(f32[4096]{0:T(1024)} %param.34) | copy-start | bytes 49156
  87.9 161.0 %all-gather.10.cloned.1.call-start = ((), (), s32[]{:S(2)}) async-start(), calls=%async_computation.8 | async-start | bytes 7864320 | tf_op jit(solution)/shard_map/all_gather | solution.py:175
  161.4 42.9 %copy-start.2 = (bf16[48,4096]{1,0:T(8,128)(2,1)}, bf16[48,4096]{1,0:T(8,128)(2,1)S(1)}, u32[]{:S(2)}) copy-start(bf16[48,4096]{1,0:T(8,128)(2,1)S(1)} %fusion.39) | copy-start | bytes 1179652
  204.3 71.5 %all-gather.8.cloned.1.call-start = ((), (), s32[]{:S(2)}) async-start(), calls=%async_computation.6 | async-start | bytes 1966080 | tf_op jit(solution)/shard_map/all_gather | solution.py:176
  204.9 189.3 %all-reduce.3.cloned.1.call-start = ((), (), s32[]{:S(2)}) async-start(), calls=%async_computation.9 | async-start | bytes 12582912
  274.5 0.7 copy-start.11
  274.5 174.5 %reduce-scatter.6.cloned.1.call-start = ((), (), s32[]{:S(2)}) async-start(), calls=%async_computation.7 | async-start | bytes 1966080 | tf_op jit(solution)/shard_map/reduce_scatter | solution.py:188
  397.5 5.8 %copy-start.9 = (f32[48,2]{0,1:T(2,128)S(1)}, f32[48,2]{0,1:T(2,128)}, u32[]{:S(2)}) copy-start(f32[48,2]{0,1:T(2,128)} %param.36) | copy-start | bytes 1156
  397.5 42.4 %all-to-all-start.1 = ((bf16[1,8,24,4096]{3,2,0,1:T(8,128)(2,1)}), bf16[1,8,24,4096]{3,2,0,1:T(8,128)(2,1)}, u32[]{:S(2)}, u32[]{:S(2)}) async-start(bf16[1,8,24,4096]{3,2,0,1:T(8,128)(2,1)} %constant_dynamic-slice_fusion), calls=%async_computation.3 | async-start | bytes 3145728 | tf_op jit(solution)/shard_map/all_to_all | solution.py:197
  445.4 4.9 %copy-start.6 = (f32[4096]{0:T(1024)S(1)}, f32[4096]{0:T(1024)}, u32[]{:S(2)}) copy-start(f32[4096]{0:T(1024)} %param.43) | copy-start | bytes 49156
Sparse Core Ops, SparseCore 0:
  9.6 47.1 all-gather.5
  88.0 70.5 reduce-scatter.3
  204.4 44.4 all-gather.9
  250.3 19.6 all-gather.7
  274.6 119.4 all-reduce.2
  396.5 28.2 reduce-scatter.5
where the time goes:
time: 460 us; the launch traced here: 459 us
  waiting for transfers between devices  270 us (59%)
  blocking collectives  75 us (16%)
  matrix products  52.1 us (11%)
  local copies, waits for them, and re-layouts  25 us (5%)
  other arithmetic  17.1 us (4%)
  between operations  13.7 us (3%)
  starting transfers between devices  6.04 us (1%)
    unnamed x7, waiting for transfers between devices  109 us
    reduce_scatter x1, waiting for transfers between devices, on_device(): lax.psum_scatter(jnp.dot(attention, out_proj, preferred_element_type=jnp....  69.8 us
    all_gather x1, waiting for transfers between devices, on_device(): column = lax.all_gather(arrived[None], 'tp', axis=0, tiled=True)  43.8 us
    all_to_all x1, blocking collectives, on_device(): lax.all_to_all(own_table, 'sp', split_axis=0, concat_axis=0, tiled=True)  42.3 us
    all_to_all x1, waiting for transfers between devices, on_device(): lax.all_to_all(routed_sum.astype(jnp.bfloat16), 'sp', split_axis=1, conca...  36.5 us
    all_gather x1, blocking collectives, on_device(): rotary_piece = lax.all_gather(key_rot, 'sp', axis=0, tiled=True)  32.8 us
    dot_general x2, matrix products, expert_block(): jnp.dot(hidden, down_part, preferred_element_type=jnp.float32)  20.1 us
    all_gather x1, waiting for transfers between devices, on_device(): latent_piece = lax.all_gather(latent_normed, 'sp', axis=0, tiled=True)  10.5 us
  transfers between devices with their start and end apart: 7, of which 5 were waited for; matrix products, arithmetic and copies ran while one was open for 12% of the time, Pallas kernels for 0%

commit v1 on v0

--- a/solution.py
+++ b/solution.py
@@ -136,7 +136,13 @@
         jnp.zeros((heads_here, local_rows, VALUE_DIM), jnp.float32),
     )
     latent_piece = lax.all_gather(latent_normed, "sp", axis=0, tiled=True)
-    rotary_piece = lax.all_gather(key_rot, "sp", axis=0, tiled=True)
+    n_dev = lax.axis_size("sp")
+    held, blocks = (key_rot, [key_rot])
+    for _ in range(n_dev - 1):
+        held = lax.ppermute(held, "sp", [(i, (i + 1) % n_dev) for i in range(n_dev)])
+        blocks.insert(0, held)
+    merged = jnp.concatenate(blocks, axis=0)
+    rotary_piece = jnp.roll(merged, (lax.axis_index("sp") + 1) * key_rot.shape[0], axis=0)
     piece_rows = latent_piece.shape[0]
     step_rows = math.gcd(piece_rows, 512)
 

time: 460 us -> 461 us (level)
  blocking collectives: 75 us -> 42.3 us
  waiting for transfers between devices: 270 us -> 299 us
    ppermute x0 -> x7, waiting for transfers between devices: none -> 41 us  [on_device(): lax.ppermute(held, 'sp', [(i, (i + 1) % n_dev) for i in range(n_dev)])]
    all_gather x1 -> x0, blocking collectives: 32.8 us -> none  [on_device(): rotary_piece = lax.all_gather(key_rot, 'sp', axis=0, tiled=True)]
    all_gather x1, waiting for transfers between devices: 10.5 us -> 0.01 us  [on_device(): latent_piece = lax.all_gather(latent_normed, 'sp', axis=0, tiled=True)]
  transfers between devices with their start and end apart: 7 -> 14, of which waited for: 5 -> 11; matrix products, arithmetic and copies ran while one was open for 12% -> 12% of each run, Pallas kernels for 0% -> 0%
where the time goes in v1:
time: 461 us; the launch traced here: 459 us
  waiting for transfers between devices  299 us (65%)
  matrix products  52 us (11%)
  blocking collectives  42.3 us (9%)
  local copies, waits for them, and re-layouts  26.1 us (6%)
  other arithmetic  17 us (4%)
  between operations  13.8 us (3%)
  starting transfers between devices  9.1 us (2%)
    unnamed x7, waiting for transfers between devices  110 us
    reduce_scatter x1, waiting for transfers between devices, on_device(): lax.psum_scatter(jnp.dot(attention, out_proj, preferred_element_type=jnp....  68.1 us
    all_gather x1, waiting for transfers between devices, on_device(): column = lax.all_gather(arrived[None], 'tp', axis=0, tiled=True)  43.8 us
    all_to_all x1, blocking collectives, on_device(): lax.all_to_all(own_table, 'sp', split_axis=0, concat_axis=0, tiled=True)  42.3 us
    ppermute x7, waiting for transfers between devices, on_device(): lax.ppermute(held, 'sp', [(i, (i + 1) % n_dev) for i in range(n_dev)])  41 us
    all_to_all x1, waiting for transfers between devices, on_device(): lax.all_to_all(routed_sum.astype(jnp.bfloat16), 'sp', split_axis=1, conca...  36.5 us
    dot_general x2, matrix products, expert_block(): jnp.dot(hidden, down_part, preferred_element_type=jnp.float32)  20.1 us
  transfers between devices with their start and end apart: 14, of which 11 were waited for; matrix products, arithmetic and copies ran while one was open for 12% of the time, Pallas kernels for 0%

profile of v1, /device:TPU:0, one launch (start us, length us, event | category | flops | bytes accessed | tf_op | source)
XLA Modules:
  0.0 459.3 jit_solution(56015200580845666)
XLA Ops:
  6.5 1.2 fusion.46
  7.8 1.7 fusion.48
  9.6 0.7 convert_element_type.118
  10.3 0.1 multiply_cosine_fusion
  10.5 3.0 collective-permute-start
  13.5 4.8 %collective-permute-done = bf16[192,32]{0,1:T(8,128)(2,1)S(1)} collective-permute-done((bf16[192,32]{0,1:T(8,128)(2,1)S(1)}, bf16[192,32]{0,1:T(8,128)(2,1)S(1)}, u32[]{:S(2)}, u32[]{:S(2)}) %collective-permute-start) | collective-permute-done | bytes 12320 | tf_op jit(solution)/shard_map/ppermute | solution.py:142
  18.3 6.5 %collective-permute-done.1 = bf16[192,32]{0,1:T(8,128)(2,1)S(1)} collective-permute-done((bf16[192,32]{0,1:T(8,128)(2,1)S(1)}, bf16[192,32]{0,1:T(8,128)(2,1)S(1)}, u32[]{:S(2)}, u32[]{:S(2)}) %collective-permute-start.1) | collective-permute-done | bytes 12320 | tf_op jit(solution)/shard_map/ppermute | solution.py:142
  24.8 6.5 %collective-permute-done.2 = bf16[192,32]{0,1:T(8,128)(2,1)S(1)} collective-permute-done((bf16[192,32]{0,1:T(8,128)(2,1)S(1)}, bf16[192,32]{0,1:T(8,128)(2,1)S(1)}, u32[]{:S(2)}, u32[]{:S(2)}) %collective-permute-start.2) | collective-permute-done | bytes 12320 | tf_op jit(solution)/shard_map/ppermute | solution.py:142
  31.3 6.4 %collective-permute-done.3 = bf16[192,32]{0,1:T(8,128)(2,1)S(1)} collective-permute-done((bf16[192,32]{0,1:T(8,128)(2,1)S(1)}, bf16[192,32]{0,1:T(8,128)(2,1)S(1)}, u32[]{:S(2)}, u32[]{:S(2)}) %collective-permute-start.3) | collective-permute-done | bytes 12320 | tf_op jit(solution)/shard_map/ppermute | solution.py:142
  37.8 1.1 copy.54
  38.9 5.7 %collective-permute-done.4 = bf16[192,32]{0,1:T(8,128)(2,1)S(1)} collective-permute-done((bf16[192,32]{0,1:T(8,128)(2,1)S(1)}, bf16[192,32]{0,1:T(8,128)(2,1)S(1)}, u32[]{:S(2)}, u32[]{:S(2)}) %collective-permute-start.4) | collective-permute-done | bytes 12320 | tf_op jit(solution)/shard_map/ppermute | solution.py:142
  44.6 6.4 %collective-permute-done.5 = bf16[192,32]{0,1:T(8,128)(2,1)S(1)} collective-permute-done((bf16[192,32]{0,1:T(8,128)(2,1)S(1)}, bf16[192,32]{0,1:T(8,128)(2,1)S(1)}, u32[]{:S(2)}, u32[]{:S(2)}) %collective-permute-start.5) | collective-permute-done | bytes 12320 | tf_op jit(solution)/shard_map/ppermute | solution.py:142
  51.1 2.0 copy.53
  53.1 4.6 %collective-permute-done.6 = bf16[192,32]{0,1:T(8,128)(2,1)S(1)} collective-permute-done((bf16[192,32]{0,1:T(8,128)(2,1)S(1)}, bf16[192,32]{0,1:T(8,128)(2,1)S(1)}, u32[]{:S(2)}, u32[]{:S(2)}) %collective-permute-start.6) | collective-permute-done | bytes 12320 | tf_op jit(solution)/shard_map/ppermute | solution.py:142
  57.7 0.1 concatenate.15
  57.9 0.7 constant_dynamic-slice_fusion.1
  58.6 1.2 broadcast_in_dim.34
  59.8 22.1 %while.18 = (s32[]{:T(128)}, f32[16,192]{1,0:T(8,128)S(1)}, f32[16,192]{1,0:T(8,128)S(1)}, f32[16,192,64]{1,2,0:T(8,128)}, s32[]{:T(128)}, /*index=5*/bf16[1536,...) while((s32[]{:T(128)}, f32[16,192]{1,0:T(8,128)S(1)}, ...), condition=%wide.region_6.7_spmd.clone, body=%wide.region_1.6_spmd.clone.sunk | while | flops 1591188224 | bytes 74948008 | solution.py:160
  59.8 22.1 %conditional.3 = ((f32[16,192]{1,0:T(8,128)S(1)}, f32[16,192]{1,0:T(8,128)S(1)}, f32[16,192,64]{1,2,0:T(8,128)})) conditional(s32[]{:T(128)} %convert_element_type.198, (f32[16,192]{1,0:T(8,128)S(1)}, f32[16,192]{1,0:T(8,128)S(1)}, f32[16,192,64]{1,2,0:T(8,128)}) %tuple.60, (s32[]{:T(128)}, s32[]{:T(128)}, bf16[1536,512]{1,0:T(8,128)(2,1)}, ...), branch_computations={%region_2.2_spmd, %region_3.5_spmd} | conditional | flops 1591188224 | bytes 74946960 | solution.py:153
  59.8 3.1 convolution_convert_fusion.1
  62.9 1.5 copy.51
  64.4 2.1 fusion.64
  66.5 0.1 broadcast_compare_fusion
  66.6 2.9 fusion.63
  69.5 1.6 fusion.5
  71.2 1.0 copy-done.1
  72.2 2.7 convolution_convert_fusion
  74.9 1.5 copy.52
  76.4 5.4 %fusion.9 = f32[16,192,64]{1,2,0:T(8,128)} fusion(bf16[512,16,64]{0,2,1:T(8,128)(2,1)S(1)} %bitcast.70, f32[16,192,512]{2,1,0:T(8,128)} %copy-done.1, f32[16,192]{1,0:T(8,128)S(1)} %max.5, f32[16,192,64]{1,2,0:T(8,128)} %get-tuple-element.325, f32[16,192]{1,0:T(8,128)S(1)} %get-tuple-element.405), kind=kOutput, calls=%fused_computation.12 | convolution fusion | flops 204865536 | bytes 8937472 | tf_op jit(solution)/shard_map/while/body/eval_jaxpr/cond/branch_1_fun/hqk,khd->hqd/dot_general | solution.py:125
  81.9 1.3 divide_convert_fusion
  83.3 6.4 %convolution_convert_fusion.5 = bf16[192,4096]{1,0:T(8,128)(2,1)} fusion(bf16[192,1024]{0,1:T(8,128)(2,1)S(1)} %bitcast.76, bf16[1024,4096]{1,0:T(8,128)(2,1)} %param.31), kind=kOutput, calls=%fused_computation.28 | convolution fusion | flops 1611399168 | bytes 10354688 | tf_op jit(solution)/shard_map/dot_general | solution.py:168
  89.7 0.1 copy.55
  89.8 0.1 eq.31
  90.0 0.1 reduce_window_sum.11
  90.2 0.2 select_reduce_fusion
  90.4 0.1 reduce_sum.74
  90.6 0.1 fusion.56
  90.7 68.1 %reduce-scatter.4.cloned.1.call-done = bf16[48,4096]{1,0:T(8,128)(2,1)} async-done(((bf16[192,4096]{1,0:T(8,128)(2,1)}), bf16[48,4096]{1,0:T(8,128)(2,1)}) %reduce-scatter.4.cloned.1.call-update) | async-done | bytes 393232 | tf_op jit(solution)/shard_map/reduce_scatter | solution.py:167
  158.8 1.2 fusion.33
  160.0 1.4 fusion.37
  161.4 0.2 fusion.39
  161.6 0.6 convolution_convert_fusion.3
  162.2 42.3 %all_to_all.10 = bf16[8,24,4096]{2,1,0:T(8,128)(2,1)} all-to-all(bf16[8,24,4096]{2,1,0:T(8,128)(2,1)S(1)} %bitcast.75), channel_id=1, replica_groups=mesh['sp'=8,'tp'=4] {'sp'}, dimensions={0} | all-to-all | bytes 3145728 | tf_op jit(solution)/shard_map/all_to_all | solution.py:180
  204.5 0.5 all-gather.7.cloned.1.call-update
  205.0 0.2 all-reduce.3.cloned.1.call-start
  205.3 43.8 %all-gather.9.cloned.1.call-done = bf16[32,24,4096]{2,1,0:T(8,128)(2,1)} async-done(((bf16[8,24,4096]{2,1,0:T(8,128)(2,1)}), bf16[32,24,4096]{2,1,0:T(8,128)(2,1)}) %all-gather.9.cloned.1.call-update) | async-done | bytes 6291472 | tf_op jit(solution)/shard_map/all_gather | solution.py:181
  249.0 6.1 %fusion.22 = f32[768,256]{1,0:T(8,128)} fusion(bf16[768,4096]{1,0:T(8,128)(2,1)} %bitcast.78, bf16[1,4096,256]{2,1,0:T(8,128)(2,1)} %param.37), kind=kOutput, calls=%fused_computation.32 | convolution fusion | flops 1610612736 | bytes 9175040 | tf_op jit(solution)/shard_map/dot_general | solution.py:43
  255.1 13.3 %convolution_convert_fusion.2 = bf16[768,4096]{1,0:T(8,128)(2,1)} fusion(bf16[1,256,4096]{2,1,0:T(8,128)(2,1)S(1)} %copy-done, bf16[768,4096]{1,0:T(8,128)(2,1)} %bitcast.79, bf16[1,4096,256]{2,1,0:T(8,128)(2,1)} %param.38, f32[768,256]{1,0:T(8,128)} %fusion.22), kind=kOutput, calls=%fused_computation.25 | convolution fusion | flops 3225550848 | bytes 17563648 | tf_op jit(solution)/shard_map/dot_general | solution.py:46
  268.4 6.2 %copy.58 = bf16[4,8,24,4096]{3,2,0,1:T(8,128)(2,1)} copy(bf16[4,8,24,4096]{3,2,1,0:T(8,128)(2,1)} %bitcast.73) | data formatting | bytes 12582912 | tf_op jit(solution)/shard_map/reshape | solution.py:189
  274.7 0.6 copy-done.10
  275.3 0.6 dynamic-slice
  275.9 2.6 fusion.65
  278.6 6.8 %convolution_convert_fusion.4 = bf16[192,4096]{1,0:T(8,128)(2,1)} fusion(bf16[256,4096]{1,0:T(8,128)(2,1)} %param.42, bf16[192,4096]{1,0:T(8,128)(2,1)} %all-gather.7.cloned.1.call-done, bf16[4096,256]{1,0:T(8,128)(2,1)} %param.41, f32[192,256]{1,0:T(8,128)S(1)} %fusion.65), kind=kOutput, calls=%fused_computation.27 | convolution fusion | flops 806387712 | bytes 7536640 | tf_op jit(solution)/shard_map/dot_general | solution.py:46
  285.4 108.9 %all-reduce.3.cloned.1.call-done = bf16[4,8,24,4096]{3,2,0,1:T(8,128)(2,1)} async-done(((bf16[4,8,24,4096]{3,2,0,1:T(8,128)(2,1)}), bf16[4,8,24,4096]{3,2,0,1:T(8,128)(2,1)}) %all-reduce.3.cloned.1.call-update) | async-done | bytes 6291472
  394.3 3.3 constant_dynamic-slice_fusion
  397.7 5.6 %all-to-all-start.1 = ((bf16[1,8,24,4096]{3,2,0,1:T(8,128)(2,1)}), bf16[1,8,24,4096]{3,2,0,1:T(8,128)(2,1)}, u32[]{:S(2)}, u32[]{:S(2)}) async-start(bf16[1,8,24,4096]{3,2,0,1:T(8,128)(2,1)} %constant_dynamic-slice_fusion), calls=%async_computation.3 | async-start | bytes 3145728 | tf_op jit(solution)/shard_map/all_to_all | solution.py:203
  403.3 0.1 mul.264
  403.5 0.1 copy.59
  403.6 36.5 %all-to-all-done.1 = bf16[1,8,24,4096]{3,2,0,1:T(8,128)(2,1)} async-done(((bf16[1,8,24,4096]{3,2,0,1:T(8,128)(2,1)}), bf16[1,8,24,4096]{3,2,0,1:T(8,128)(2,1)}, u32[]{:S(2)}, u32[]{:S(2)}) %all-to-all-start.1) | async-done | bytes 1572896 | tf_op jit(solution)/shard_map/all_to_all | solution.py:203
  440.0 3.4 gather_fusion
  443.4 2.1 reshape.251
  445.6 3.6 multiply_reduce_fusion
  449.2 1.2 multiply_reduce_fusion.1
  450.5 1.9 fusion.40
  (65 shorter events, 0.7 us)
Async XLA Ops:
  6.5 248.6 %copy-start = (bf16[1,256,4096]{2,1,0:T(8,128)(2,1)S(1)}, bf16[1,256,4096]{2,1,0:T(8,128)(2,1)}, u32[]{:S(2)}) copy-start(bf16[1,256,4096]{2,1,0:T(8,128)(2,1)} %param.39) | copy-start | bytes 6291460
  6.5 52.1 %all-gather.5.cloned.1.call-start = ((), (), s32[]{:S(2)}) async-start(), calls=%async_computation.4 | async-start | bytes 1769472 | tf_op jit(solution)/shard_map/all_gather | solution.py:138
  9.5 149.3 %reduce-scatter.4.cloned.1.call-start = ((), (), s32[]{:S(2)}) async-start(), calls=%async_computation.5 | async-start | bytes 1966080 | tf_op jit(solution)/shard_map/reduce_scatter | solution.py:167
  10.5 7.8 %collective-permute-start = (bf16[192,32]{0,1:T(8,128)(2,1)S(1)}, bf16[192,32]{0,1:T(8,128)(2,1)S(1)}, u32[]{:S(2)}, u32[]{:S(2)}) collective-permute-start(bf16[192,32]{0,1:T(8,128)(2,1)S(1)} %pad_maximum_fusion.1), channel_id=1, source_target_pairs={{0,4},{4,8},{8,12},{12,16},{16,20},{20,24},{24,28},{28,0},{1,5},{5... | collective-permute-start | bytes 36872 | tf_op jit(solution)/shard_map/ppermute | solution.py:142
  18.3 6.5 %collective-permute-start.1 = (bf16[192,32]{0,1:T(8,128)(2,1)S(1)}, bf16[192,32]{0,1:T(8,128)(2,1)S(1)}, u32[]{:S(2)}, u32[]{:S(2)}) collective-permute-start(bf16[192,32]{0,1:T(8,128)(2,1)S(1)} %collective-permute-done), channel_id=1, source_target_pairs={{0,4},{4,8},{8,12},{12,16},{16,20},{20,24},{24,28},{28,0},{1,5},{5... | collective-permute-start | bytes 36872 | tf_op jit(solution)/shard_map/ppermute | solution.py:142
  24.8 6.5 %collective-permute-start.2 = (bf16[192,32]{0,1:T(8,128)(2,1)S(1)}, bf16[192,32]{0,1:T(8,128)(2,1)S(1)}, u32[]{:S(2)}, u32[]{:S(2)}) collective-permute-start(bf16[192,32]{0,1:T(8,128)(2,1)S(1)} %collective-permute-done.1), channel_id=1, source_target_pairs={{0,4},{4,8},{8,12},{12,16},{16,20},{20,24},{24,28},{28,0},{1,5},{5... | collective-permute-start | bytes 36872 | tf_op jit(solution)/shard_map/ppermute | solution.py:142
  31.3 6.4 %collective-permute-start.3 = (bf16[192,32]{0,1:T(8,128)(2,1)S(1)}, bf16[192,32]{0,1:T(8,128)(2,1)S(1)}, u32[]{:S(2)}, u32[]{:S(2)}) collective-permute-start(bf16[192,32]{0,1:T(8,128)(2,1)S(1)} %collective-permute-done.2), channel_id=1, source_target_pairs={{0,4},{4,8},{8,12},{12,16},{16,20},{20,24},{24,28},{28,0},{1,5},{5... | collective-permute-start | bytes 36872 | tf_op jit(solution)/shard_map/ppermute | solution.py:142
  37.8 6.8 %collective-permute-start.4 = (bf16[192,32]{0,1:T(8,128)(2,1)S(1)}, bf16[192,32]{0,1:T(8,128)(2,1)S(1)}, u32[]{:S(2)}, u32[]{:S(2)}) collective-permute-start(bf16[192,32]{0,1:T(8,128)(2,1)S(1)} %collective-permute-done.3), channel_id=1, source_target_pairs={{0,4},{4,8},{8,12},{12,16},{16,20},{20,24},{24,28},{28,0},{1,5},{5... | collective-permute-start | bytes 36872 | tf_op jit(solution)/shard_map/ppermute | solution.py:142
  44.5 6.5 %collective-permute-start.5 = (bf16[192,32]{0,1:T(8,128)(2,1)S(1)}, bf16[192,32]{0,1:T(8,128)(2,1)S(1)}, u32[]{:S(2)}, u32[]{:S(2)}) collective-permute-start(bf16[192,32]{0,1:T(8,128)(2,1)S(1)} %collective-permute-done.4), channel_id=1, source_target_pairs={{0,4},{4,8},{8,12},{12,16},{16,20},{20,24},{24,28},{28,0},{1,5},{5... | collective-permute-start | bytes 36872 | tf_op jit(solution)/shard_map/ppermute | solution.py:142
  51.1 6.7 %collective-permute-start.6 = (bf16[192,32]{0,1:T(8,128)(2,1)S(1)}, bf16[192,32]{0,1:T(8,128)(2,1)S(1)}, u32[]{:S(2)}, u32[]{:S(2)}) collective-permute-start(bf16[192,32]{0,1:T(8,128)(2,1)S(1)} %collective-permute-done.5), channel_id=1, source_target_pairs={{0,4},{4,8},{8,12},{12,16},{16,20},{20,24},{24,28},{28,0},{1,5},{5... | collective-permute-start | bytes 36872 | tf_op jit(solution)/shard_map/ppermute | solution.py:142
  69.5 2.7 copy-start.1
  69.5 2.7 copy-start.9
  83.2 6.5 %copy-start.7 = (s32[48,2]{0,1:T(2,128)S(1)}, s32[48,2]{0,1:T(2,128)}, u32[]{:S(2)}) copy-start(s32[48,2]{0,1:T(2,128)} %param.35) | copy-start | bytes 1156
  89.6 70.3 %copy-start.3 = (bf16[48,4096]{1,0:T(8,128)(2,1)S(1)}, bf16[48,4096]{1,0:T(8,128)(2,1)}, u32[]{:S(2)}) copy-start(bf16[48,4096]{1,0:T(8,128)(2,1)} %param.32) | copy-start | bytes 1179652
  89.6 70.3 %copy-start.4 = (f32[4096]{0:T(1024)S(1)}, f32[4096]{0:T(1024)}, u32[]{:S(2)}) copy-start(f32[4096]{0:T(1024)} %param.33) | copy-start | bytes 49156
  89.6 71.7 %copy-start.6 = (f32[4096]{0:T(1024)S(1)}, f32[4096]{0:T(1024)}, u32[]{:S(2)}) copy-start(f32[4096]{0:T(1024)} %param.34) | copy-start | bytes 49156
  89.7 159.4 %all-gather.9.cloned.1.call-start = ((), (), s32[]{:S(2)}) async-start(), calls=%async_computation.8 | async-start | bytes 7864320 | tf_op jit(solution)/shard_map/all_gather | solution.py:181
  161.5 42.9 %copy-start.2 = (bf16[48,4096]{1,0:T(8,128)(2,1)}, bf16[48,4096]{1,0:T(8,128)(2,1)S(1)}, u32[]{:S(2)}) copy-start(bf16[48,4096]{1,0:T(8,128)(2,1)S(1)} %fusion.39) | copy-start | bytes 1179652
  204.5 71.5 %all-gather.7.cloned.1.call-start = ((), (), s32[]{:S(2)}) async-start(), calls=%async_computation.6 | async-start | bytes 1966080 | tf_op jit(solution)/shard_map/all_gather | solution.py:182
  205.0 189.3 %all-reduce.3.cloned.1.call-start = ((), (), s32[]{:S(2)}) async-start(), calls=%async_computation.9 | async-start | bytes 12582912
  274.7 0.7 copy-start.10
  274.7 174.5 %reduce-scatter.6.cloned.1.call-start = ((), (), s32[]{:S(2)}) async-start(), calls=%async_computation.7 | async-start | bytes 1966080 | tf_op jit(solution)/shard_map/reduce_scatter | solution.py:194
  397.7 5.8 %copy-start.8 = (f32[48,2]{0,1:T(2,128)S(1)}, f32[48,2]{0,1:T(2,128)}, u32[]{:S(2)}) copy-start(f32[48,2]{0,1:T(2,128)} %param.36) | copy-start | bytes 1156
  397.7 42.4 %all-to-all-start.1 = ((bf16[1,8,24,4096]{3,2,0,1:T(8,128)(2,1)}), bf16[1,8,24,4096]{3,2,0,1:T(8,128)(2,1)}, u32[]{:S(2)}, u32[]{:S(2)}) async-start(bf16[1,8,24,4096]{3,2,0,1:T(8,128)(2,1)} %constant_dynamic-slice_fusion), calls=%async_computation.3 | async-start | bytes 3145728 | tf_op jit(solution)/shard_map/all_to_all | solution.py:203
  445.6 4.9 %copy-start.5 = (f32[4096]{0:T(1024)S(1)}, f32[4096]{0:T(1024)}, u32[]{:S(2)}) copy-start(f32[4096]{0:T(1024)} %param.43) | copy-start | bytes 49156
Sparse Core Ops, SparseCore 0:
  9.6 46.8 all-gather.4
  89.8 68.9 reduce-scatter.3
  204.6 44.4 all-gather.8
  250.5 19.6 all-gather.6
  274.8 119.4 all-reduce.2
  396.7 28.2 reduce-scatter.5
